TPU v7x, 32 devices: a whole 2x2x4 slice. The times are simulated.
32 devices in a mesh: sp: 4 (over x, core), dp: 8 (over z, y).
Axes of the slice: x: 2, y: 2, z: 4, core: 2. Of those that a mesh axis runs over, the one named last changes fastest.
Arguments:
- queries: bfloat16 [16, 8, 576, 128], P('dp', None, 'sp'), may hold values from -6 to 6
- keys: bfloat16 [16, 8, 576, 128], P('dp', None, 'sp'), may hold values from -6 to 6
- values: bfloat16 [16, 8, 576, 128], P('dp', None, 'sp'), may hold values from -6 to 6
- in_gate: bfloat16 [16, 8, 576], P('dp', None, 'sp'), may hold values from -5 to 240
- forget_gate: bfloat16 [16, 8, 576], P('dp', None, 'sp'), may hold values from 1 to 20
- out_gate: bfloat16 [16, 8, 576, 128], P('dp', None, 'sp'), may hold values from -6 to 6
- norm_gain: float32 [8, 128], replicated, may hold values from 0.1 to 1.9
- out_weight: bfloat16 [1024, 2048], P(None, 'dp'), may hold values from -0.1875 to 0.1875
Outputs:
- mixed: bfloat16 [16, 576, 2048], P('dp', 'sp')
All inputs are finite; a program needn't handle non-finite values.
Results may differ from a plain program's by a relative error of at most 0.0057.
Values may be sent and summed in bfloat16 or wider, within the bound.
A program may use at most 64 MiB of HBM per device.

v0:
```python
import jax
import jax.numpy as jnp
from jax import lax
from jax.sharding import PartitionSpec as P

BLK = 64
highest = lax.Precision.HIGHEST
norm_eps = 1e-05


def run_cells(parts):
    query_in, key_in, value_in, input_in, forget_in = parts
    item_count = query_in.shape[1]
    seq_len = query_in.shape[2]
    head_size = query_in.shape[3]
    blocks = seq_len // BLK
    key_scale = head_size ** (-0.5)
    query_b = query_in.reshape(item_count, blocks, BLK, head_size)
    key_b = key_in.reshape(item_count, blocks, BLK, head_size)
    value_b = value_in.reshape(item_count, blocks, BLK, head_size)
    input_b = input_in.astype(jnp.float32).reshape(item_count, blocks, BLK)
    logf_b = jax.nn.log_sigmoid(forget_in.astype(jnp.float32)).reshape(item_count, blocks, BLK)
    cumulative = jnp.cumsum(logf_b, axis=-1)
    block_end = cumulative[..., -1]
    growth = block_end[..., None] - cumulative + input_b
    growth_max = jnp.max(growth, axis=-1)
    w_key = jnp.exp(growth - growth_max[..., None]) * key_scale
    key_f = key_b.astype(jnp.float32)
    value_f = value_b.astype(jnp.float32)
    weighted = w_key[..., None] * key_f
    fresh_memory = jnp.einsum("ncsd,ncse->ncde", weighted, value_f, precision=highest)
    fresh_norm = jnp.sum(weighted, axis=2)

    def advance(state_in, inputs):
        memory, normalizer, stabilizer = state_in
        end_now, top_now, memory_add, norm_add = inputs
        stab_new = jnp.maximum(end_now + stabilizer, top_now)
        decay_old = jnp.exp(end_now + stabilizer - stab_new)
        decay_add = jnp.exp(top_now - stab_new)
        memory_new = decay_old[:, None, None] * memory + decay_add[:, None, None] * memory_add
        norm_new = decay_old[:, None] * normalizer + decay_add[:, None] * norm_add
        return ((memory_new, norm_new, stab_new), (memory, normalizer, stabilizer))

    start = (
        jnp.zeros((item_count, head_size, head_size), jnp.float32),
        jnp.zeros((item_count, head_size), jnp.float32),
        jnp.zeros((item_count,), jnp.float32),
    )
    series = (
        jnp.swapaxes(block_end, 0, 1),
        jnp.swapaxes(growth_max, 0, 1),
        jnp.swapaxes(fresh_memory, 0, 1),
        jnp.swapaxes(fresh_norm, 0, 1),
    )
    _, (memory_prev, norm_prev, stab_prev) = lax.scan(advance, start, series)
    memory_prev = jnp.swapaxes(memory_prev, 0, 1)
    norm_prev = jnp.swapaxes(norm_prev, 0, 1)
    stab_prev = jnp.swapaxes(stab_prev, 0, 1)
    causal_mask = jnp.tril(jnp.ones((BLK, BLK), dtype=bool))
    log_weights = cumulative[..., :, None] - cumulative[..., None, :] + input_b[..., None, :]
    log_weights = jnp.where(causal_mask, log_weights, -jnp.inf)
    carried_log = cumulative + stab_prev[..., None]
    row_max = jnp.maximum(jnp.max(log_weights, axis=-1), carried_log)
    w_intra = jnp.exp(log_weights - row_max[..., None])
    w_inter = jnp.exp(carried_log - row_max)
    scores = jnp.einsum("ncpd,ncqd->ncpq", query_b, key_b, preferred_element_type=jnp.float32) * (
        key_scale * w_intra
    )
    query_f = query_b.astype(jnp.float32)
    numerator = w_inter[..., None] * jnp.einsum(
        "ncpd,ncde->ncpe", query_f, memory_prev, precision=highest
    )
    numerator = numerator + jnp.einsum("ncpq,ncqe->ncpe", scores, value_f, precision=highest)
    denominator = w_inter * jnp.einsum(
        "ncpd,ncd->ncp", query_f, norm_prev, precision=highest
    ) + jnp.sum(scores, axis=-1)
    cell_out = numerator / jnp.maximum(jnp.abs(denominator), 1.0)[..., None]
    return cell_out.reshape(1, item_count, seq_len, head_size).astype(jnp.bfloat16)


def body(queries, keys, values, in_gate, forget_gate, out_gate, norm_gain, out_weight):
    rank_count = lax.axis_size("sp")
    group_seqs, head_count, span_len, head_size = queries.shape

    def by_rank(array):
        return array.reshape((rank_count, -1) + array.shape[2:])

    cell_out = run_cells(
        (
            lax.all_to_all(by_rank(queries), "sp", split_axis=0, concat_axis=2, tiled=True),
            lax.all_to_all(by_rank(keys), "sp", split_axis=0, concat_axis=2, tiled=True),
            lax.all_to_all(by_rank(values), "sp", split_axis=0, concat_axis=2, tiled=True),
            lax.all_to_all(by_rank(in_gate), "sp", split_axis=0, concat_axis=2, tiled=True),
            lax.all_to_all(by_rank(forget_gate), "sp", split_axis=0, concat_axis=2, tiled=True),
        )
    )
    returned = lax.all_to_all(cell_out, "sp", split_axis=2, concat_axis=0, tiled=True)
    returned = returned.reshape(group_seqs, head_count, span_len, head_size).astype(jnp.float32)
    mean_val = jnp.mean(returned, axis=-1, keepdims=True)
    centered = returned - mean_val
    variance = jnp.mean(centered * centered, axis=-1, keepdims=True)
    normed = centered * lax.rsqrt(variance + norm_eps) * norm_gain[None, :, None, :]
    hidden = (normed * jax.nn.sigmoid(out_gate.astype(jnp.float32))).astype(jnp.bfloat16)
    hidden = jnp.swapaxes(hidden, 1, 2).reshape(group_seqs * span_len, head_count * head_size)
    result = jnp.dot(
        hidden,
        lax.all_gather(out_weight, "dp", axis=1, tiled=True),
        preferred_element_type=jnp.float32,
    )
    return result.astype(jnp.bfloat16).reshape(group_seqs, span_len, -1)


def solution(mesh):
    return jax.shard_map(
        body,
        mesh=mesh,
        in_specs=(
            P("dp", None, "sp", None),
            P("dp", None, "sp", None),
            P("dp", None, "sp", None),
            P("dp", None, "sp"),
            P("dp", None, "sp"),
            P("dp", None, "sp", None),
            P(),
            P(None, "dp"),
        ),
        out_specs=P("dp", "sp", None),
        check_vma=False,
    )
```

profile of v0, /device:TPU:0, one launch (start us, length us, event | category | flops | bytes accessed | tf_op | source)
XLA Modules:
  0.0 103.2 jit_solution(3290982956562113304)
XLA Ops:
  6.5 1.3 %reshape.170 = bf16[4,4,144]{2,1,0:T(4,128)(2,1)} reshape(bf16[2,8,144]{2,1,0:T(8,128)(2,1)} %param.14) | data formatting | bytes 9216 | tf_op jit(solution)/shard_map/reshape | solution.py:86
  7.8 4.2 %all-to-all-start = ((bf16[4,4,144]{2,1,0:T(4,128)(2,1)}), bf16[4,4,144]{2,1,0:T(4,128)(2,1)S(1)}, u32[]{:S(2)}, u32[]{:S(2)}) async-start(bf16[4,4,144]{2,1,0:T(4,128)(2,1)} %reshape.170), calls=%async_computation | async-start | bytes 16384 | tf_op jit(solution)/shard_map/all_to_all | solution.py:94
  12.1 0.7 all-gather.2.cloned.1.call-update
  12.9 1.3 %reshape.171 = bf16[4,4,144]{2,1,0:T(4,128)(2,1)} reshape(bf16[2,8,144]{2,1,0:T(8,128)(2,1)} %param.13) | data formatting | bytes 9216 | tf_op jit(solution)/shard_map/reshape | solution.py:86
  14.2 1.7 %all-to-all-done = bf16[4,4,144]{2,1,0:T(4,128)(2,1)S(1)} async-done(((bf16[4,4,144]{2,1,0:T(4,128)(2,1)}), bf16[4,4,144]{2,1,0:T(4,128)(2,1)S(1)}, u32[]{:S(2)}, u32[]{:S(2)}) %all-to-all-start) | async-done | bytes 4640 | tf_op jit(solution)/shard_map/all_to_all | solution.py:94
  15.9 3.2 %all-to-all-start.1 = ((bf16[4,4,144]{2,1,0:T(4,128)(2,1)}), bf16[4,4,144]{2,1,0:T(4,128)(2,1)S(1)}, u32[]{:S(2)}, u32[]{:S(2)}) async-start(bf16[4,4,144]{2,1,0:T(4,128)(2,1)} %reshape.171), calls=%async_computation.1 | async-start | bytes 16384 | tf_op jit(solution)/shard_map/all_to_all | solution.py:93
  19.2 3.8 %all-to-all-done.1 = bf16[4,4,144]{2,1,0:T(4,128)(2,1)S(1)} async-done(((bf16[4,4,144]{2,1,0:T(4,128)(2,1)}), bf16[4,4,144]{2,1,0:T(4,128)(2,1)S(1)}, u32[]{:S(2)}, u32[]{:S(2)}) %all-to-all-start.1) | async-done | bytes 4640 | tf_op jit(solution)/shard_map/all_to_all | solution.py:93
  22.9 3.5 %all-to-all-start.2 = ((bf16[4,4,144,128]{3,2,1,0:T(8,128)(2,1)}), bf16[4,4,144,128]{3,2,1,0:T(8,128)(2,1)S(1)}, u32[]{:S(2)}, u32[]{:S(2)}) async-start(bf16[4,4,144,128]{3,2,1,0:T(8,128)(2,1)} %bitcast.130), calls=%async_computation.2 | async-start | bytes 1179648 | tf_op jit(solution)/shard_map/all_to_all | solution.py:91
  26.5 0.1 neg.37
  26.5 0.1 reshape.180
  26.7 0.9 reduce_window_sum.11
  27.6 0.2 slice_reduce_fusion
  27.7 8.2 %all-to-all-done.2 = bf16[4,4,144,128]{3,2,1,0:T(8,128)(2,1)S(1)} async-done(((bf16[4,4,144,128]{3,2,1,0:T(8,128)(2,1)}), bf16[4,4,144,128]{3,2,1,0:T(8,128)(2,1)S(1)}, u32[]{:S(2)}, u32[]{:S(2)}) %all-to-all-start.2) | async-done | bytes 589856 | tf_op jit(solution)/shard_map/all_to_all | solution.py:91
  35.9 3.5 %all-to-all-start.3 = ((bf16[4,4,144,128]{3,2,1,0:T(8,128)(2,1)}), bf16[4,4,144,128]{3,2,1,0:T(8,128)(2,1)S(1)}, u32[]{:S(2)}, u32[]{:S(2)}) async-start(bf16[4,4,144,128]{3,2,1,0:T(8,128)(2,1)} %bitcast.10), calls=%async_computation.3 | async-start | bytes 1179648 | tf_op jit(solution)/shard_map/all_to_all | solution.py:92
  39.4 0.2 fusion.29
  39.6 0.1 copy.72
  39.7 0.1 copy.71
  39.7 0.8 fusion.16
  40.5 0.1 exponential_multiply_fusion
  40.7 8.2 %all-to-all-done.3 = bf16[4,4,144,128]{3,2,1,0:T(8,128)(2,1)S(1)} async-done(((bf16[4,4,144,128]{3,2,1,0:T(8,128)(2,1)}), bf16[4,4,144,128]{3,2,1,0:T(8,128)(2,1)S(1)}, u32[]{:S(2)}, u32[]{:S(2)}) %all-to-all-start.3) | async-done | bytes 589856 | tf_op jit(solution)/shard_map/all_to_all | solution.py:92
  48.9 4.2 %all-to-all-start.4 = ((bf16[4,4,144,128]{3,2,1,0:T(8,128)(2,1)}), bf16[4,4,144,128]{3,2,1,0:T(8,128)(2,1)}, u32[]{:S(2)}, u32[]{:S(2)}) async-start(bf16[4,4,144,128]{3,2,1,0:T(8,128)(2,1)} %bitcast.18), calls=%async_computation.4 | async-start | bytes 1179648 | tf_op jit(solution)/shard_map/all_to_all | solution.py:90
  53.1 0.4 fusion.17
  53.5 2.4 %convolution_bitcast_fusion = f32[9,4,128,128]{3,2,0,1:T(8,128)S(1)} fusion(bf16[4,9,64,128]{3,2,1,0:T(8,128)(2,1)S(1)} %bitcast.123, bf16[4,9,64,128]{3,2,1,0:T(8,128)(2,1)S(1)} %bitcast.120, f32[4,9,64]{2,1,0:T(8,128)S(1)} %exponential_multiply_fusion), kind=kOutput, calls=%fused_computation.19 | convolution fusion | flops 453574656 | bytes 3548160 | tf_op jit(solution)/shard_map/ncsd,ncse->ncde/dot_general | solution.py:31
  55.9 9.3 %while.21 = (s32[]{:T(128)}, f32[4,128,128]{2,1,0:T(8,128)S(1)}, f32[4,128]{1,0:T(4,128)S(1)}, f32[4]{0:T(128)S(1)}, f32[9,4,128,128]{3,2,1,0:T(8,128)}, /*index...) while((s32[]{:T(128)}, f32[4,128,128]{2,1,0:T(8,128)S(1)}, ...), condition=%wide.region_4.5_spmd.clone, body=%wide.region_3.4_spmd.clone.sunk | while | flops 330263 | bytes 1325971 | solution.py:55
  56.0 0.7 bitcast_dynamic-update-slice_fusion.4
  56.7 0.1 fusion.42
  56.8 0.1 multiply_add_fusion.2
  57.0 0.7 bitcast_dynamic-update-slice_fusion.4
  57.7 0.1 fusion.42
  58.0 0.7 bitcast_dynamic-update-slice_fusion.4
  58.7 0.1 fusion.42
  58.9 0.1 multiply_add_fusion.2
  59.0 0.7 bitcast_dynamic-update-slice_fusion.4
  59.8 0.1 fusion.42
  59.9 0.1 multiply_add_fusion.2
  60.1 0.7 bitcast_dynamic-update-slice_fusion.4
  60.8 0.1 fusion.42
  61.0 0.1 multiply_add_fusion.2
  61.1 0.7 bitcast_dynamic-update-slice_fusion.4
  61.9 0.1 fusion.42
  62.2 0.7 bitcast_dynamic-update-slice_fusion.4
  62.9 0.1 fusion.42
  63.2 0.7 bitcast_dynamic-update-slice_fusion.4
  63.9 0.1 fusion.42
  64.2 0.7 bitcast_dynamic-update-slice_fusion.4
  65.0 0.1 fusion.42
  65.2 0.1 copy.75
  65.3 1.1 %copy.76 = bf16[1,4,4,144,128]{4,3,2,1,0:T(8,128)(2,1)S(1)} copy(bf16[1,4,4,144,128]{4,3,1,2,0:T(8,128)(2,1)} %bitcast.20) | data formatting | bytes 1179648 | tf_op jit(solution)/shard_map/all_to_all | solution.py:90
  66.5 1.0 fusion.27
  67.5 0.7 fusion.31
  68.3 0.1 fusion.26
  68.4 0.9 copy-done.2
  69.2 1.3 %fusion.11 = f32[4,9,64,128]{3,2,1,0:T(8,128)S(1)} fusion(bf16[4,9,64,128]{3,2,1,0:T(8,128)(2,1)S(1)} %bitcast.129, f32[4,9,64]{2,1,0:T(8,128)S(1)} %get-tuple-element.183, f32[9,4,128,128]{3,2,1,0:T(8,128)S(1)} %copy-done.2), kind=kOutput, calls=%fused_computation.21 | convolution fusion | flops 453279744 | bytes 4137984 | tf_op jit(solution)/shard_map/ncpd,ncde->ncpe/dot_general | solution.py:70
  70.6 1.3 %fusion.15 = bf16[4,9,64,128]{3,2,1,0:T(8,128)(2,1)S(1)} fusion(f32[4,9,64,128]{3,2,1,0:T(8,128)S(1)} %fusion.11, f32[4,9,64,64]{2,3,1,0:T(8,128)S(1)} %get-tuple-element.186, bf16[4,9,64,128]{3,2,1,0:T(8,128)(2,1)S(1)} %bitcast.124, f32[4,9,64]{2,1,0:T(8,128)S(1)} %get-tuple-element.182), kind=kOutput, calls=%fused_computation.25 | convolution fusion | flops 227377152 | bytes 2958336 | tf_op jit(solution)/shard_map/ncpq,ncqe->ncpe/dot_general | solution.py:73
  71.9 0.5 copy.79
  72.4 12.6 %all_to_all.72 = bf16[1,4,576,128]{3,1,0,2:T(4,128)(2,1)S(1)} all-to-all(bf16[1,4,576,128]{3,1,0,2:T(4,128)(2,1)S(1)} %copy.79), channel_id=1, replica_groups=mesh['sp'=4,'dp'=8] {'sp'}, dimensions={2} | all-to-all | bytes 1179648 | tf_op jit(solution)/shard_map/all_to_all | solution.py:97
  85.1 0.7 fusion.18
  85.8 0.2 copy.91
  86.0 1.4 %multiply_reduce_fusion = f32[4,4,144]{1,2,0:T(8,128)S(1)} fusion(bf16[1,4,4,144,128]{4,1,3,2,0:T(4,128)(2,1)S(1)} %bitcast.118, f32[4,4,144]{1,2,0:T(8,128)S(1)} %broadcast_multiply_fusion), kind=kLoop, calls=%fused_computation.28 | loop fusion | flops 1177344 | bytes 608256 | tf_op jit(solution)/shard_map/reduce_sum | solution.py:101
  87.5 0.2 copy.92
  87.8 0.8 fusion.22
  88.6 0.2 copy.84
  88.7 3.1 %all-gather.2.cloned.1.call-done = bf16[1024,2048]{1,0:T(8,128)(2,1)} async-done(((bf16[1024,256]{1,0:T(8,128)(2,1)}), bf16[1024,2048]{1,0:T(8,128)(2,1)}) %all-gather.2.cloned.1.call-update) | async-done | bytes 4194320 | tf_op jit(solution)/shard_map/all_gather | solution.py:107
  91.8 4.6 %convolution_convert_fusion = bf16[288,2048]{1,0:T(8,128)(2,1)} fusion(bf16[1024,2048]{1,0:T(8,128)(2,1)} %all-gather.2.cloned.1.call-done, bf16[36,8,8,128]{3,2,1,0:T(8,128)(2,1)S(1)} %bitcast.131), kind=kOutput, calls=%fused_computation.16 | convolution fusion | flops 1208549376 | bytes 5963776 | tf_op jit(solution)/shard_map/dot_general | solution.py:105
  (82 shorter events, 1.7 us)
Async XLA Ops:
  7.8 8.1 %all-to-all-start = ((bf16[4,4,144]{2,1,0:T(4,128)(2,1)}), bf16[4,4,144]{2,1,0:T(4,128)(2,1)S(1)}, u32[]{:S(2)}, u32[]{:S(2)}) async-start(bf16[4,4,144]{2,1,0:T(4,128)(2,1)} %reshape.170), calls=%async_computation | async-start | bytes 16384 | tf_op jit(solution)/shard_map/all_to_all | solution.py:94
  12.1 79.7 %all-gather.2.cloned.1.call-start = ((), (), s32[]{:S(2)}) async-start(), calls=%async_computation.6 | async-start | bytes 4718592 | tf_op jit(solution)/shard_map/all_gather | solution.py:107
  15.9 7.0 %all-to-all-start.1 = ((bf16[4,4,144]{2,1,0:T(4,128)(2,1)}), bf16[4,4,144]{2,1,0:T(4,128)(2,1)S(1)}, u32[]{:S(2)}, u32[]{:S(2)}) async-start(bf16[4,4,144]{2,1,0:T(4,128)(2,1)} %reshape.171), calls=%async_computation.1 | async-start | bytes 16384 | tf_op jit(solution)/shard_map/all_to_all | solution.py:93
  22.9 13.0 %all-to-all-start.2 = ((bf16[4,4,144,128]{3,2,1,0:T(8,128)(2,1)}), bf16[4,4,144,128]{3,2,1,0:T(8,128)(2,1)S(1)}, u32[]{:S(2)}, u32[]{:S(2)}) async-start(bf16[4,4,144,128]{3,2,1,0:T(8,128)(2,1)} %bitcast.130), calls=%async_computation.2 | async-start | bytes 1179648 | tf_op jit(solution)/shard_map/all_to_all | solution.py:91
  35.9 13.0 %all-to-all-start.3 = ((bf16[4,4,144,128]{3,2,1,0:T(8,128)(2,1)}), bf16[4,4,144,128]{3,2,1,0:T(8,128)(2,1)S(1)}, u32[]{:S(2)}, u32[]{:S(2)}) async-start(bf16[4,4,144,128]{3,2,1,0:T(8,128)(2,1)} %bitcast.10), calls=%async_computation.3 | async-start | bytes 1179648 | tf_op jit(solution)/shard_map/all_to_all | solution.py:92
  48.9 16.4 %all-to-all-start.4 = ((bf16[4,4,144,128]{3,2,1,0:T(8,128)(2,1)}), bf16[4,4,144,128]{3,2,1,0:T(8,128)(2,1)}, u32[]{:S(2)}, u32[]{:S(2)}) async-start(bf16[4,4,144,128]{3,2,1,0:T(8,128)(2,1)} %bitcast.18), calls=%async_computation.4 | async-start | bytes 1179648 | tf_op jit(solution)/shard_map/all_to_all | solution.py:90
  53.1 2.8 %copy-start = (bf16[1,4,4,144,128]{4,3,2,1,0:T(8,128)(2,1)}, bf16[1,4,4,144,128]{4,3,2,1,0:T(8,128)(2,1)S(1)}, u32[]{:S(2)}) copy-start(bf16[1,4,4,144,128]{4,3,2,1,0:T(8,128)(2,1)S(1)} %copy.70) | copy-start | bytes 1769476
  67.5 1.7 %copy-start.2 = (f32[9,4,128,128]{3,2,1,0:T(8,128)S(1)}, f32[9,4,128,128]{3,2,1,0:T(8,128)}, u32[]{:S(2)}) copy-start(f32[9,4,128,128]{3,2,1,0:T(8,128)} %get-tuple-element.65) | copy-start | bytes 7077892
  69.2 1.3 %copy-start.1 = (bf16[1,4,4,144,128]{4,3,2,1,0:T(8,128)(2,1)S(1)}, bf16[1,4,4,144,128]{4,3,2,1,0:T(8,128)(2,1)}, u32[]{:S(2)}) copy-start(bf16[1,4,4,144,128]{4,3,2,1,0:T(8,128)(2,1)} %copy-done) | copy-start | bytes 1769476
  85.8 1.9 %copy-start.3 = (bf16[2,8,144,128]{3,2,1,0:T(8,128)(2,1)S(1)}, bf16[2,8,144,128]{3,2,1,0:T(8,128)(2,1)}, u32[]{:S(2)}) copy-start(bf16[2,8,144,128]{3,2,1,0:T(8,128)(2,1)} %param.15) | copy-start | bytes 1769476
  85.8 1.9 %copy-start.4 = (f32[8,128]{1,0:T(8,128)S(1)}, f32[8,128]{1,0:T(8,128)}, u32[]{:S(2)}) copy-start(f32[8,128]{1,0:T(8,128)} %param.16) | copy-start | bytes 12292
Sparse Core Ops, SparseCore 0:
  14.9 76.8 all-gather.1
where the time goes:
time: 104 us; the launch traced here: 103 us
  waiting for transfers between devices  25.6 us (25%)
  starting transfers between devices  18.6 us (18%)
  other arithmetic  14.3 us (14%)
  between operations  13.7 us (13%)
  blocking collectives  12.6 us (12%)
  matrix products  11.4 us (11%)
  local copies, waits for them, and re-layouts  6.74 us (6%)
    all_to_all x1, blocking collectives, body(): lax.all_to_all(cell_out, 'sp', split_axis=2, concat_axis=0, tiled=True)  12.6 us
    all_to_all x1, waiting for transfers between devices, body(): lax.all_to_all(by_rank(keys), 'sp', split_axis=0, concat_axis=2, tiled=True)  8.19 us
    all_to_all x1, waiting for transfers between devices, body(): lax.all_to_all(by_rank(values), 'sp', split_axis=0, concat_axis=2, tiled=...  8.19 us
    dynamic_update_slice x18, other arithmetic, run_cells(): _, (memory_prev, norm_prev, stab_prev) = lax.scan(advance, start, series)  6.71 us
    dot_general x1, matrix products, body(): jnp.dot(hidden, lax.all_gather(out_weight, 'dp', axis=1, tiled=True), pre...  4.59 us
    all_to_all x1, starting transfers between devices, body(): lax.all_to_all(by_rank(forget_gate), 'sp', split_axis=0, concat_axis=2, t...  4.24 us
    all_to_all x1, starting transfers between devices, body(): lax.all_to_all(by_rank(queries), 'sp', split_axis=0, concat_axis=2, tiled...  4.15 us
    all_to_all x1, waiting for transfers between devices, body(): lax.all_to_all(by_rank(in_gate), 'sp', split_axis=0, concat_axis=2, tiled...  3.76 us
  transfers between devices with their start and end apart: 6, of which 5 were waited for; matrix products, arithmetic and copies ran while one was open for 25% of the time, Pallas kernels for 0%

commit v1 on v0

--- a/solution.py
+++ b/solution.py
@@ -1,3 +1,4 @@
+import functools
 import jax
 import jax.numpy as jnp
 from jax import lax
@@ -6,6 +7,41 @@
 BLK = 64
 highest = lax.Precision.HIGHEST
 norm_eps = 1e-05
+
+
+def order_the_slices(mine, at_axis, incoming_x):
+    block_last = mine.shape
+    current_value = mine.reshape(
+        *block_last[:at_axis],
+        incoming_x,
+        block_last[at_axis] // incoming_x,
+        *block_last[at_axis + 1 :]
+    )
+    return jnp.moveaxis(current_value, at_axis, 0)
+
+
+def fill_the_orders(local, k_dim):
+    r1 = list(local.shape[1:])
+    r1[k_dim] *= local.shape[0]
+    return jnp.moveaxis(local, 0, k_dim).reshape(r1)
+
+
+def recast_rails(block_in, bus_axis, field, work_x):
+    raw_out = jax.lax.psum(1, axis_name=bus_axis)
+    mid_arr, y = (raw_out, jax.lax.axis_index(bus_axis))
+    taken_in = order_the_slices(block_in, field, mid_arr)
+    inter = taken_in
+    for i in range(1, mid_arr):
+        v_now, d_next = ((y + i) % mid_arr, (y - i) % mid_arr)
+        out_arr = lax.dynamic_index_in_dim(taken_in, v_now, 0)
+        block_next = jax.lax.ppermute(
+            out_arr, bus_axis, [(u, (u + i) % mid_arr) for u in range(mid_arr)]
+        )
+        inter = lax.dynamic_update_slice_in_dim(inter, block_next, d_next, axis=0)
+    return fill_the_orders(inter, work_x)
+
+
+_obtain_series_all = functools.partial(recast_rails, bus_axis="sp", field=0, work_x=2)
 
 
 def run_cells(parts):
@@ -91,7 +127,7 @@
             lax.all_to_all(by_rank(keys), "sp", split_axis=0, concat_axis=2, tiled=True),
             lax.all_to_all(by_rank(values), "sp", split_axis=0, concat_axis=2, tiled=True),
             lax.all_to_all(by_rank(in_gate), "sp", split_axis=0, concat_axis=2, tiled=True),
-            lax.all_to_all(by_rank(forget_gate), "sp", split_axis=0, concat_axis=2, tiled=True),
+            _obtain_series_all(by_rank(forget_gate)),
         )
     )
     returned = lax.all_to_all(cell_out, "sp", split_axis=2, concat_axis=0, tiled=True)

time: 104 us -> 108 us (1.038)
  waiting for transfers between devices: 25.6 us -> 29.5 us
    all_gather x1, waiting for transfers between devices: 3.06 us -> 9.7 us  [body(): lax.all_gather(out_weight, 'dp', axis=1, tiled=True)]
    ppermute x0 -> x3, starting transfers between devices: none -> 4.48 us  [recast_rails(): jax.lax.ppermute(out_arr, bus_axis, [(u, (u + i) % mid_arr) for u in rang...]
    all_to_all x1 -> x0, starting transfers between devices: 4.24 us -> none  [body(): lax.all_to_all(by_rank(forget_gate), 'sp', split_axis=0, concat_axis=2, t...]
    all_to_all x1 -> x0, waiting for transfers between devices: 1.71 us -> none  [body(): lax.all_to_all(by_rank(forget_gate), 'sp', split_axis=0, concat_axis=2, t...]
    reshape x2 -> x1, local copies, waits for them, and re-layouts: 2.61 us -> 1.3 us  [by_rank(): return array.reshape((rank_count, -1) + array.shape[2:])]
    all_to_all x1, waiting for transfers between devices: 3.76 us -> 2.62 us  [body(): lax.all_to_all(by_rank(in_gate), 'sp', split_axis=0, concat_axis=2, tiled...]
  transfers between devices with their start and end apart: 6 -> 8, of which waited for: 5 -> 4; matrix products, arithmetic and copies ran while one was open for 25% -> 24% of each run, Pallas kernels for 0% -> 0%
where the time goes in v1:
time: 108 us; the launch traced here: 107 us
  waiting for transfers between devices  29.5 us (27%)
  starting transfers between devices  18.9 us (17%)
  other arithmetic  14.3 us (13%)
  between operations  13.8 us (13%)
  blocking collectives  12.6 us (12%)
  matrix products  11.4 us (11%)
  local copies, waits for them, and re-layouts  6.3 us (6%)
    all_to_all x1, blocking collectives, body(): lax.all_to_all(cell_out, 'sp', split_axis=2, concat_axis=0, tiled=True)  12.6 us
    all_gather x1, waiting for transfers between devices, body(): lax.all_gather(out_weight, 'dp', axis=1, tiled=True)  9.7 us
    all_to_all x1, waiting for transfers between devices, body(): lax.all_to_all(by_rank(values), 'sp', split_axis=0, concat_axis=2, tiled=...  8.28 us
    all_to_all x1, waiting for transfers between devices, body(): lax.all_to_all(by_rank(keys), 'sp', split_axis=0, concat_axis=2, tiled=True)  8.18 us
    dynamic_update_slice x18, other arithmetic, run_cells(): _, (memory_prev, norm_prev, stab_prev) = lax.scan(advance, start, series)  6.75 us
    dot_general x1, matrix products, body(): jnp.dot(hidden, lax.all_gather(out_weight, 'dp', axis=1, tiled=True), pre...  4.59 us
    ppermute x3, starting transfers between devices, recast_rails(): jax.lax.ppermute(out_arr, bus_axis, [(u, (u + i) % mid_arr) for u in rang...  4.48 us
    all_to_all x1, starting transfers between devices, body(): lax.all_to_all(by_rank(queries), 'sp', split_axis=0, concat_axis=2, tiled...  4.15 us
  transfers between devices with their start and end apart: 8, of which 4 were waited for; matrix products, arithmetic and copies ran while one was open for 24% of the time, Pallas kernels for 0%

profile of v1, /device:TPU:0, one launch (start us, length us, event | category | flops | bytes accessed | tf_op | source)
XLA Modules:
  0.0 107.1 jit_solution(5731189011787389597)
XLA Ops:
  6.5 0.7 reshape_reshape.3
  7.3 0.5 collective-permute-start
  7.8 2.6 %collective-permute-start.1 = (bf16[1,1,4,144]{3,0,2,1:T(2,128)(2,1)S(1)}, bf16[1,1,4,144]{3,0,2,1:T(2,128)(2,1)S(1)}, u32[]{:S(2)}, u32[]{:S(2)}) collective-permute-start(bf16[1,1,4,144]{3,0,2,1:T(2,128)(2,1)S(1)} %get-tuple-element.186), channel_id=1, source_target_pairs={{0,16},{8,24},{16,0},{24,8},{1,17},{9,25},{17,1},{25,9},{2,18},{10... | collective-permute-start | bytes 3464 | tf_op jit(solution)/shard_map/ppermute | solution.py:37
  10.4 1.4 %collective-permute-start.2 = (bf16[1,1,4,144]{3,0,2,1:T(2,128)(2,1)S(1)}, bf16[1,1,4,144]{3,0,2,1:T(2,128)(2,1)S(1)}, u32[]{:S(2)}, u32[]{:S(2)}) collective-permute-start(bf16[1,1,4,144]{3,0,2,1:T(2,128)(2,1)S(1)} %get-tuple-element.185), channel_id=1, source_target_pairs={{0,24},{8,0},{16,8},{24,16},{1,25},{9,1},{17,9},{25,17},{2,26},{10... | collective-permute-start | bytes 3464 | tf_op jit(solution)/shard_map/ppermute | solution.py:37
  11.8 1.3 %reshape.166 = bf16[4,4,144]{2,1,0:T(4,128)(2,1)} reshape(bf16[2,8,144]{2,1,0:T(8,128)(2,1)} %param.13) | data formatting | bytes 9216 | tf_op jit(solution)/shard_map/reshape | solution.py:122
  13.1 3.2 %all-to-all-start = ((bf16[4,4,144]{2,1,0:T(4,128)(2,1)}), bf16[4,4,144]{2,1,0:T(4,128)(2,1)S(1)}, u32[]{:S(2)}, u32[]{:S(2)}) async-start(bf16[4,4,144]{2,1,0:T(4,128)(2,1)} %reshape.166), calls=%async_computation | async-start | bytes 16384 | tf_op jit(solution)/shard_map/all_to_all | solution.py:129
  16.4 0.7 all-gather.2.cloned.1.call-update
  17.4 0.1 neg.33
  17.5 2.6 %all-to-all-done = bf16[4,4,144]{2,1,0:T(4,128)(2,1)S(1)} async-done(((bf16[4,4,144]{2,1,0:T(4,128)(2,1)}), bf16[4,4,144]{2,1,0:T(4,128)(2,1)S(1)}, u32[]{:S(2)}, u32[]{:S(2)}) %all-to-all-start) | async-done | bytes 4640 | tf_op jit(solution)/shard_map/all_to_all | solution.py:129
  20.1 3.5 %all-to-all-start.1 = ((bf16[4,4,144,128]{3,2,1,0:T(8,128)(2,1)}), bf16[4,4,144,128]{3,2,1,0:T(8,128)(2,1)S(1)}, u32[]{:S(2)}, u32[]{:S(2)}) async-start(bf16[4,4,144,128]{3,2,1,0:T(8,128)(2,1)} %bitcast.128), calls=%async_computation.1 | async-start | bytes 1179648 | tf_op jit(solution)/shard_map/all_to_all | solution.py:127
  23.6 0.9 reduce_window_sum.11
  24.5 0.2 slice_reduce_fusion
  24.7 0.1 copy.83
  24.8 0.1 reshape.175
  24.9 8.2 %all-to-all-done.1 = bf16[4,4,144,128]{3,2,1,0:T(8,128)(2,1)S(1)} async-done(((bf16[4,4,144,128]{3,2,1,0:T(8,128)(2,1)}), bf16[4,4,144,128]{3,2,1,0:T(8,128)(2,1)S(1)}, u32[]{:S(2)}, u32[]{:S(2)}) %all-to-all-start.1) | async-done | bytes 589856 | tf_op jit(solution)/shard_map/all_to_all | solution.py:127
  33.1 3.5 %all-to-all-start.2 = ((bf16[4,4,144,128]{3,2,1,0:T(8,128)(2,1)}), bf16[4,4,144,128]{3,2,1,0:T(8,128)(2,1)S(1)}, u32[]{:S(2)}, u32[]{:S(2)}) async-start(bf16[4,4,144,128]{3,2,1,0:T(8,128)(2,1)} %bitcast.9), calls=%async_computation.2 | async-start | bytes 1179648 | tf_op jit(solution)/shard_map/all_to_all | solution.py:128
  36.6 0.2 fusion.29
  36.7 0.1 copy.84
  36.8 0.8 fusion.16
  37.6 0.1 exponential_multiply_fusion
  37.8 8.3 %all-to-all-done.2 = bf16[4,4,144,128]{3,2,1,0:T(8,128)(2,1)S(1)} async-done(((bf16[4,4,144,128]{3,2,1,0:T(8,128)(2,1)}), bf16[4,4,144,128]{3,2,1,0:T(8,128)(2,1)S(1)}, u32[]{:S(2)}, u32[]{:S(2)}) %all-to-all-start.2) | async-done | bytes 589856 | tf_op jit(solution)/shard_map/all_to_all | solution.py:128
  46.1 4.2 %all-to-all-start.3 = ((bf16[4,4,144,128]{3,2,1,0:T(8,128)(2,1)}), bf16[4,4,144,128]{3,2,1,0:T(8,128)(2,1)}, u32[]{:S(2)}, u32[]{:S(2)}) async-start(bf16[4,4,144,128]{3,2,1,0:T(8,128)(2,1)} %bitcast.17), calls=%async_computation.3 | async-start | bytes 1179648 | tf_op jit(solution)/shard_map/all_to_all | solution.py:126
  50.3 0.4 fusion.17
  50.7 2.4 %convolution_bitcast_fusion = f32[9,4,128,128]{3,2,0,1:T(8,128)S(1)} fusion(bf16[4,9,64,128]{3,2,1,0:T(8,128)(2,1)S(1)} %bitcast.121, bf16[4,9,64,128]{3,2,1,0:T(8,128)(2,1)S(1)} %bitcast.118, f32[4,9,64]{2,1,0:T(8,128)S(1)} %exponential_multiply_fusion), kind=kOutput, calls=%fused_computation.19 | convolution fusion | flops 453574656 | bytes 3548160 | tf_op jit(solution)/shard_map/ncsd,ncse->ncde/dot_general | solution.py:67
  53.1 9.4 %while.21 = (s32[]{:T(128)}, f32[4,128,128]{2,1,0:T(8,128)S(1)}, f32[4,128]{1,0:T(4,128)S(1)}, f32[4]{0:T(128)S(1)}, f32[9,4,128,128]{3,2,1,0:T(8,128)}, /*index...) while((s32[]{:T(128)}, f32[4,128,128]{2,1,0:T(8,128)S(1)}, ...), condition=%wide.region_4.5_spmd.clone, body=%wide.region_3.4_spmd.clone.sunk | while | flops 330263 | bytes 1325971 | solution.py:91
  53.1 0.7 bitcast_dynamic-update-slice_fusion.4
  53.8 0.1 fusion.42
  54.0 0.1 multiply_add_fusion.2
  54.1 0.7 bitcast_dynamic-update-slice_fusion.4
  54.9 0.1 fusion.42
  55.0 0.1 multiply_add_fusion.2
  55.2 0.7 bitcast_dynamic-update-slice_fusion.4
  55.9 0.1 fusion.42
  56.0 0.1 multiply_add_fusion.2
  56.2 0.7 bitcast_dynamic-update-slice_fusion.4
  56.9 0.1 fusion.42
  57.2 0.7 bitcast_dynamic-update-slice_fusion.4
  58.0 0.1 fusion.42
  58.3 0.7 bitcast_dynamic-update-slice_fusion.4
  59.0 0.1 fusion.42
  59.3 0.7 bitcast_dynamic-update-slice_fusion.4
  60.1 0.1 fusion.42
  60.4 0.7 bitcast_dynamic-update-slice_fusion.4
  61.1 0.1 fusion.42
  61.4 0.7 bitcast_dynamic-update-slice_fusion.4
  62.2 0.1 fusion.42
  62.4 0.1 copy.87
  62.5 1.1 %copy.88 = bf16[1,4,4,144,128]{4,3,2,1,0:T(8,128)(2,1)S(1)} copy(bf16[1,4,4,144,128]{4,3,1,2,0:T(8,128)(2,1)} %bitcast.19) | data formatting | bytes 1179648 | tf_op jit(solution)/shard_map/all_to_all | solution.py:126
  63.7 1.0 fusion.27
  64.7 0.7 fusion.31
  65.5 0.1 fusion.26
  65.6 0.8 copy-done.2
  66.4 1.3 %fusion.11 = f32[4,9,64,128]{3,2,1,0:T(8,128)S(1)} fusion(bf16[4,9,64,128]{3,2,1,0:T(8,128)(2,1)S(1)} %bitcast.127, f32[4,9,64]{2,1,0:T(8,128)S(1)} %get-tuple-element.183, f32[9,4,128,128]{3,2,1,0:T(8,128)S(1)} %copy-done.2), kind=kOutput, calls=%fused_computation.21 | convolution fusion | flops 453279744 | bytes 4137984 | tf_op jit(solution)/shard_map/ncpd,ncde->ncpe/dot_general | solution.py:106
  67.7 1.3 %fusion.15 = bf16[4,9,64,128]{3,2,1,0:T(8,128)(2,1)S(1)} fusion(f32[4,9,64,128]{3,2,1,0:T(8,128)S(1)} %fusion.11, f32[4,9,64,64]{2,3,1,0:T(8,128)S(1)} %get-tuple-element.189, bf16[4,9,64,128]{3,2,1,0:T(8,128)(2,1)S(1)} %bitcast.122, f32[4,9,64]{2,1,0:T(8,128)S(1)} %get-tuple-element.182), kind=kOutput, calls=%fused_computation.25 | convolution fusion | flops 227377152 | bytes 2958336 | tf_op jit(solution)/shard_map/ncpq,ncqe->ncpe/dot_general | solution.py:109
  69.1 0.5 copy.91
  69.5 12.6 %all_to_all.63 = bf16[1,4,576,128]{3,1,0,2:T(4,128)(2,1)S(1)} all-to-all(bf16[1,4,576,128]{3,1,0,2:T(4,128)(2,1)S(1)} %copy.91), channel_id=1, replica_groups=mesh['sp'=4,'dp'=8] {'sp'}, dimensions={2} | all-to-all | bytes 1179648 | tf_op jit(solution)/shard_map/all_to_all | solution.py:133
  82.3 0.7 fusion.18
  83.0 0.2 copy.103
  83.2 1.4 %multiply_reduce_fusion = f32[4,4,144]{1,2,0:T(8,128)S(1)} fusion(bf16[1,4,4,144,128]{4,1,3,2,0:T(4,128)(2,1)S(1)} %bitcast.116, f32[4,4,144]{1,2,0:T(8,128)S(1)} %broadcast_multiply_fusion), kind=kLoop, calls=%fused_computation.28 | loop fusion | flops 1177344 | bytes 608256 | tf_op jit(solution)/shard_map/reduce_sum | solution.py:137
  84.7 0.2 copy.104
  85.0 0.8 fusion.22
  85.8 0.2 copy.96
  85.9 9.7 %all-gather.2.cloned.1.call-done = bf16[1024,2048]{1,0:T(8,128)(2,1)} async-done(((bf16[1024,256]{1,0:T(8,128)(2,1)}), bf16[1024,2048]{1,0:T(8,128)(2,1)}) %all-gather.2.cloned.1.call-update) | async-done | bytes 4194320 | tf_op jit(solution)/shard_map/all_gather | solution.py:143
  95.6 4.6 %convolution_convert_fusion = bf16[288,2048]{1,0:T(8,128)(2,1)} fusion(bf16[1024,2048]{1,0:T(8,128)(2,1)} %all-gather.2.cloned.1.call-done, bf16[36,8,8,128]{3,2,1,0:T(8,128)(2,1)S(1)} %bitcast.129), kind=kOutput, calls=%fused_computation.16 | convolution fusion | flops 1208549376 | bytes 5963776 | tf_op jit(solution)/shard_map/dot_general | solution.py:141
  (90 shorter events, 2.0 us)
Async XLA Ops:
  7.3 9.9 %collective-permute-start = (bf16[1,1,4,144]{3,0,2,1:T(2,128)(2,1)S(1)}, bf16[1,1,4,144]{3,0,2,1:T(2,128)(2,1)S(1)}, u32[]{:S(2)}, u32[]{:S(2)}) collective-permute-start(bf16[1,1,4,144]{3,0,2,1:T(2,128)(2,1)S(1)} %get-tuple-element.187), channel_id=1, source_target_pairs={{0,8},{8,16},{16,24},{24,0},{1,9},{9,17},{17,25},{25,1},{2,10},{10... | collective-permute-start | bytes 3464 | tf_op jit(solution)/shard_map/ppermute | solution.py:37
  7.8 9.5 %collective-permute-start.1 = (bf16[1,1,4,144]{3,0,2,1:T(2,128)(2,1)S(1)}, bf16[1,1,4,144]{3,0,2,1:T(2,128)(2,1)S(1)}, u32[]{:S(2)}, u32[]{:S(2)}) collective-permute-start(bf16[1,1,4,144]{3,0,2,1:T(2,128)(2,1)S(1)} %get-tuple-element.186), channel_id=1, source_target_pairs={{0,16},{8,24},{16,0},{24,8},{1,17},{9,25},{17,1},{25,9},{2,18},{10... | collective-permute-start | bytes 3464 | tf_op jit(solution)/shard_map/ppermute | solution.py:37
  10.4 7.0 %collective-permute-start.2 = (bf16[1,1,4,144]{3,0,2,1:T(2,128)(2,1)S(1)}, bf16[1,1,4,144]{3,0,2,1:T(2,128)(2,1)S(1)}, u32[]{:S(2)}, u32[]{:S(2)}) collective-permute-start(bf16[1,1,4,144]{3,0,2,1:T(2,128)(2,1)S(1)} %get-tuple-element.185), channel_id=1, source_target_pairs={{0,24},{8,0},{16,8},{24,16},{1,25},{9,1},{17,9},{25,17},{2,26},{10... | collective-permute-start | bytes 3464 | tf_op jit(solution)/shard_map/ppermute | solution.py:37
  13.1 7.0 %all-to-all-start = ((bf16[4,4,144]{2,1,0:T(4,128)(2,1)}), bf16[4,4,144]{2,1,0:T(4,128)(2,1)S(1)}, u32[]{:S(2)}, u32[]{:S(2)}) async-start(bf16[4,4,144]{2,1,0:T(4,128)(2,1)} %reshape.166), calls=%async_computation | async-start | bytes 16384 | tf_op jit(solution)/shard_map/all_to_all | solution.py:129
  16.3 79.3 %all-gather.2.cloned.1.call-start = ((), (), s32[]{:S(2)}) async-start(), calls=%async_computation.5 | async-start | bytes 4718592 | tf_op jit(solution)/shard_map/all_gather | solution.py:143
  20.1 13.0 %all-to-all-start.1 = ((bf16[4,4,144,128]{3,2,1,0:T(8,128)(2,1)}), bf16[4,4,144,128]{3,2,1,0:T(8,128)(2,1)S(1)}, u32[]{:S(2)}, u32[]{:S(2)}) async-start(bf16[4,4,144,128]{3,2,1,0:T(8,128)(2,1)} %bitcast.128), calls=%async_computation.1 | async-start | bytes 1179648 | tf_op jit(solution)/shard_map/all_to_all | solution.py:127
  33.1 13.0 %all-to-all-start.2 = ((bf16[4,4,144,128]{3,2,1,0:T(8,128)(2,1)}), bf16[4,4,144,128]{3,2,1,0:T(8,128)(2,1)S(1)}, u32[]{:S(2)}, u32[]{:S(2)}) async-start(bf16[4,4,144,128]{3,2,1,0:T(8,128)(2,1)} %bitcast.9), calls=%async_computation.2 | async-start | bytes 1179648 | tf_op jit(solution)/shard_map/all_to_all | solution.py:128
  46.1 16.5 %all-to-all-start.3 = ((bf16[4,4,144,128]{3,2,1,0:T(8,128)(2,1)}), bf16[4,4,144,128]{3,2,1,0:T(8,128)(2,1)}, u32[]{:S(2)}, u32[]{:S(2)}) async-start(bf16[4,4,144,128]{3,2,1,0:T(8,128)(2,1)} %bitcast.17), calls=%async_computation.3 | async-start | bytes 1179648 | tf_op jit(solution)/shard_map/all_to_all | solution.py:126
  50.3 2.8 %copy-start = (bf16[1,4,4,144,128]{4,3,2,1,0:T(8,128)(2,1)}, bf16[1,4,4,144,128]{4,3,2,1,0:T(8,128)(2,1)S(1)}, u32[]{:S(2)}) copy-start(bf16[1,4,4,144,128]{4,3,2,1,0:T(8,128)(2,1)S(1)} %copy.82) | copy-start | bytes 1769476
  64.7 1.7 %copy-start.2 = (f32[9,4,128,128]{3,2,1,0:T(8,128)S(1)}, f32[9,4,128,128]{3,2,1,0:T(8,128)}, u32[]{:S(2)}) copy-start(f32[9,4,128,128]{3,2,1,0:T(8,128)} %get-tuple-element.65) | copy-start | bytes 7077892
  66.4 1.3 %copy-start.1 = (bf16[1,4,4,144,128]{4,3,2,1,0:T(8,128)(2,1)S(1)}, bf16[1,4,4,144,128]{4,3,2,1,0:T(8,128)(2,1)}, u32[]{:S(2)}) copy-start(bf16[1,4,4,144,128]{4,3,2,1,0:T(8,128)(2,1)} %copy-done) | copy-start | bytes 1769476
  83.0 1.9 %copy-start.3 = (bf16[2,8,144,128]{3,2,1,0:T(8,128)(2,1)S(1)}, bf16[2,8,144,128]{3,2,1,0:T(8,128)(2,1)}, u32[]{:S(2)}) copy-start(bf16[2,8,144,128]{3,2,1,0:T(8,128)(2,1)} %param.15) | copy-start | bytes 1769476
  83.0 1.9 %copy-start.4 = (f32[8,128]{1,0:T(8,128)S(1)}, f32[8,128]{1,0:T(8,128)}, u32[]{:S(2)}) copy-start(f32[8,128]{1,0:T(8,128)} %param.16) | copy-start | bytes 12292
Sparse Core Ops, SparseCore 0:
  19.2 76.3 all-gather.1
